TPU v7x, 32 devices: a whole 2x2x4 slice. The times are simulated.
32 devices in a mesh: grp: 2 (over y), fs: 4 (over z), tp: 4 (over x, core).
Axes of the slice: x: 2, y: 2, z: 4, core: 2. Of those that a mesh axis runs over, the one named last changes fastest.
Arguments:
- tokens: bfloat16 [4096, 2048], P(('grp', 'fs')), parts along dimension 0, may hold values from -6 to 6
- norm_in: bfloat16 [2048], replicated, may hold values from 0.099609375 to 1.8984375
- w_value: bfloat16 [2048, 2048], P('fs', 'tp'), may hold values from -0.125 to 0.125
- w_gate: bfloat16 [2048, 2048], P('fs', 'tp'), may hold values from -0.125 to 0.125
- conv_kernel: float32 [31, 2048], replicated, as said below
- ln_gain: bfloat16 [2048], replicated, may hold values from 0.099609375 to 1.8984375
- ln_shift: bfloat16 [2048], replicated, may hold values from -3 to 3
- w_out: bfloat16 [2048, 2048], P('tp', 'fs'), may hold values from -0.125 to 0.125
- norm_mlp: bfloat16 [2048], replicated, may hold values from 0.099609375 to 1.8984375
- w_up: bfloat16 [2048, 8192], P('fs', 'tp'), may hold values from -0.125 to 0.125
- w_down: bfloat16 [8192, 2048], P('tp', 'fs'), may hold values from -0.0625 to 0.0625
Outputs:
- layer_out: bfloat16 [4096, 2048], P(('grp', 'fs', 'tp')), parts along dimension 0
There are 2 independent parts, one for each index of `grp`. A program takes and returns all parts, laid end to end along the dimension named above; an argument that names none is the same for every part. Nothing has to cross between parts.
Inputs may be any that keep to these rules, and one draw needn't show every extreme that they name: `conv_kernel`: a depthwise kernel.
All inputs are finite; a program needn't handle non-finite values.
Results may differ from a plain program's by a relative error of at most 0.018.
Values may be sent and summed in bfloat16 or wider, within the bound.
A program may use at most 64 MiB of HBM per device.

v0:
```python
import jax
import jax.numpy as jnp
from jax import lax
from jax.sharding import PartitionSpec as P

D = 2048
KERNEL = 31


def rms_scale(values, gain):
    as_float = values.astype(jnp.float32)
    scaled = as_float * lax.rsqrt(jnp.mean(as_float * as_float, axis=-1, keepdims=True) + 1e-06)
    return scaled * gain.astype(jnp.float32)


def shards(
    tokens, norm_in, w_value, w_gate, conv_kernel, ln_gain, ln_shift, w_out, norm_mlp, w_up, w_down
):
    seq_len = tokens.shape[0]
    col_width = w_value.shape[1]
    offset = lax.axis_index("tp") * col_width
    row_share = seq_len // lax.axis_size("tp")
    own_start = lax.axis_index("tp") * row_share
    normed_in = rms_scale(tokens, norm_in).astype(jnp.bfloat16)
    columns = normed_in
    values_f = jnp.dot(
        columns,
        lax.all_gather(w_value, "fs", axis=0, tiled=True),
        preferred_element_type=jnp.float32,
    )
    gate_act = jnp.dot(
        columns,
        lax.all_gather(w_gate, "fs", axis=0, tiled=True),
        preferred_element_type=jnp.float32,
    )
    gated = values_f * jax.nn.sigmoid(gate_act)
    kernel = lax.dynamic_slice_in_dim(conv_kernel, offset, col_width, 1)
    padded = jnp.pad(gated, ((KERNEL - 1, 0), (0, 0)))
    convolved = jnp.zeros_like(gated)
    for tap_index in range(KERNEL):
        convolved = convolved + kernel[tap_index][None, :] * padded[tap_index : tap_index + seq_len]
    stats = lax.psum((jnp.sum(convolved, axis=1), jnp.sum(convolved * convolved, axis=1)), "tp")
    chan_mean = (stats[0] / D)[:, None]
    chan_msq = (stats[1] / D)[:, None]
    variance = chan_msq - chan_mean * chan_mean
    gain_part = lax.dynamic_slice_in_dim(ln_gain, offset, col_width, 0).astype(jnp.float32)
    shift_part = lax.dynamic_slice_in_dim(ln_shift, offset, col_width, 0).astype(jnp.float32)
    normed = (convolved - chan_mean) * lax.rsqrt(variance + 1e-05) * gain_part + shift_part
    activated = jax.nn.silu(normed).astype(jnp.bfloat16)
    partial_value = jnp.dot(
        activated,
        lax.all_gather(w_out, "fs", axis=1, tiled=True),
        preferred_element_type=jnp.float32,
    )
    mixed = lax.psum(partial_value.astype(jnp.bfloat16), "tp").astype(jnp.float32)
    residual = tokens.astype(jnp.float32) + mixed
    normed_mlp = rms_scale(residual, norm_mlp).astype(jnp.bfloat16)
    residual_own = lax.dynamic_slice_in_dim(residual, own_start, row_share, 0)
    columns = normed_mlp
    up_act = jnp.dot(
        columns, lax.all_gather(w_up, "fs", axis=0, tiled=True), preferred_element_type=jnp.float32
    )
    hidden = jnp.square(jax.nn.relu(up_act)).astype(jnp.bfloat16)
    whole_down = lax.all_gather(w_down, "fs", axis=1, tiled=True)
    mlp_own = lax.psum_scatter(
        jnp.dot(hidden, whole_down, preferred_element_type=jnp.float32).astype(jnp.bfloat16),
        "tp",
        scatter_dimension=0,
        tiled=True,
    ).astype(jnp.float32)
    return (residual_own + mlp_own).astype(jnp.bfloat16)


def solution(mesh):
    in_specs = (
        P(("grp", "fs"), None),
        P(),
        P("fs", "tp"),
        P("fs", "tp"),
        P(),
        P(),
        P(),
        P("tp", "fs"),
        P(),
        P("fs", "tp"),
        P("tp", "fs"),
    )
    out_specs = P(("grp", "fs", "tp"), None)
    return jax.shard_map(shards, mesh=mesh, in_specs=in_specs, out_specs=out_specs, check_vma=False)
```

profile of v0, /device:TPU:0, one launch (start us, length us, event | category | flops | bytes accessed | tf_op | source)
XLA Modules:
  0.0 559.9 jit_solution(14983291080787817863)
XLA Ops:
  6.5 0.0 copy-start
  6.5 0.0 all-gather.8.cloned.1.call-start
  6.5 0.7 all-gather.8.cloned.1.call-update
  7.3 0.0 all-gather.6.cloned.1.call-start
  7.3 0.7 all-gather.6.cloned.1.call-update
  8.0 0.0 all-gather.10.cloned.1.call-start
  8.1 0.7 all-gather.10.cloned.1.call-update
  8.7 0.0 all-reduce.4.cloned.1.call-start
  8.8 0.7 convert_element_type.46
  9.5 0.8 dynamic-slice_convert_fusion
  10.3 1.1 fusion.50
  11.4 1.4 constant_dynamic-slice_fusion
  12.8 2.1 fusion
  14.8 42.5 %all-gather.8.cloned.1.call-done = bf16[2048,512]{1,0:T(8,128)(2,1)} async-done(((bf16[512,512]{1,0:T(8,128)(2,1)}), bf16[2048,512]{1,0:T(8,128)(2,1)}) %all-gather.8.cloned.1.call-update) | async-done | bytes 2097168 | tf_op jit(solution)/shard_map/all_gather | solution.py:33
  57.3 0.0 copy-done
  57.3 3.0 fusion.7
  60.4 43.0 %all-gather.6.cloned.1.call-done = bf16[2048,512]{1,0:T(8,128)(2,1)} async-done(((bf16[512,512]{1,0:T(8,128)(2,1)}), bf16[2048,512]{1,0:T(8,128)(2,1)}) %all-gather.6.cloned.1.call-update) | async-done | bytes 2097168 | tf_op jit(solution)/shard_map/all_gather | solution.py:28
  103.4 2.9 convolution_multiply_fusion
  106.3 5.0 fusion.49
  111.3 6.8 %all-reduce.1 = (f32[512]{0:T(512)S(1)}, f32[512]{0:T(512)S(1)}) all-reduce(f32[512]{0:T(512)S(1)} %get-tuple-element.6, f32[512]{0:T(512)S(1)} %get-tuple-element.5), channel_id=1, replica_groups=mesh['grp'=2,'fs'=4,'tp'=4] {'tp'}, use_global_device_ids=true, to_apply=%region_4.5 | all-reduce | flops 1024 | bytes 8192 | tf_op jit(solution)/shard_map/psum | solution.py:42
  118.1 31.4 %all-gather.10.cloned.1.call-done = bf16[512,2048]{1,0:T(8,128)(2,1)} async-done(((bf16[512,512]{1,0:T(8,128)(2,1)}), bf16[512,2048]{1,0:T(8,128)(2,1)}) %all-gather.10.cloned.1.call-update) | async-done | bytes 2097168 | tf_op jit(solution)/shard_map/all_gather | solution.py:52
  149.4 4.4 convolution_convert_fusion.1
  153.9 0.0 all-reduce.4.cloned.1.call-update
  153.9 0.0 copy-start.1
  153.9 0.0 all-gather.12.cloned.1.call-start
  153.9 0.5 all-gather.12.cloned.1.call-update
  154.5 0.0 all-gather.14.cloned.1.call-start
  154.5 0.5 all-gather.14.cloned.1.call-update
  155.1 0.2 reduce-scatter.2.cloned.1.call-start
  155.3 0.0 copy-done.1
  155.3 48.9 %all-reduce.4.cloned.1.call-done = bf16[512,2048]{1,0:T(8,128)(2,1)} async-done(((bf16[512,2048]{1,0:T(8,128)(2,1)}), bf16[512,2048]{1,0:T(8,128)(2,1)}) %all-reduce.4.cloned.1.call-update) | async-done | bytes 2097168 | tf_op jit(solution)/shard_map/psum | solution.py:55
  204.2 4.2 convert_add_fusion
  208.4 146.9 %all-gather.12.cloned.1.call-done = bf16[2048,2048]{1,0:T(8,128)(2,1)} async-done(((bf16[512,2048]{1,0:T(8,128)(2,1)}), bf16[2048,2048]{1,0:T(8,128)(2,1)}) %all-gather.12.cloned.1.call-update) | async-done | bytes 8388624 | tf_op jit(solution)/shard_map/all_gather | solution.py:61
  355.4 149.3 %all-gather.14.cloned.1.call-done = bf16[2048,2048]{1,0:T(8,128)(2,1)} async-done(((bf16[2048,512]{1,0:T(8,128)(2,1)}), bf16[2048,2048]{1,0:T(8,128)(2,1)}) %all-gather.14.cloned.1.call-update) | async-done | bytes 8388624 | tf_op jit(solution)/shard_map/all_gather | solution.py:64
  504.6 16.6 %convolution_convert_fusion = bf16[512,2048]{1,0:T(8,128)(2,1)} fusion(bf16[2048,2048]{1,0:T(8,128)(2,1)} %all-gather.14.cloned.1.call-done, bf16[2048,2048]{1,0:T(8,128)(2,1)} %all-gather.12.cloned.1.call-done, f32[2048]{0:T(1024)S(1)} %convert_element_type.53, f32[512]{0:T(512)S(1)} %add_rsqrt_fusion, bf16[512,2048]{1,0:T(8,128)(2,1)S(1)} %copy-done, ...), kind=kOutput, calls=%fused_computation.9 | convolution fusion | flops 8600420352 | bytes 23078912 | tf_op jit(solution)/shard_map/dot_general | solution.py:66
  521.2 0.0 reduce-scatter.2.cloned.1.call-update
  521.2 29.5 %reduce-scatter.2.cloned.1.call-done = bf16[128,2048]{1,0:T(8,128)(2,1)} async-done(((bf16[512,2048]{1,0:T(8,128)(2,1)}), bf16[128,2048]{1,0:T(8,128)(2,1)}) %reduce-scatter.2.cloned.1.call-update) | async-done | bytes 524304 | tf_op jit(solution)/shard_map/reduce_scatter | solution.py:65
  550.8 2.3 add_convert_fusion
  (4 shorter events, 0.0 us)
Async XLA Ops:
  6.5 50.8 %copy-start = (bf16[512,2048]{1,0:T(8,128)(2,1)S(1)}, bf16[512,2048]{1,0:T(8,128)(2,1)}, u32[]{:S(2)}) copy-start(bf16[512,2048]{1,0:T(8,128)(2,1)} %param.11) | copy-start | bytes 6291460
  6.5 50.8 %all-gather.8.cloned.1.call-start = ((), (), s32[]{:S(2)}) async-start(), calls=%async_computation.2 | async-start | bytes 2621440 | tf_op jit(solution)/shard_map/all_gather | solution.py:33
  7.3 96.1 %all-gather.6.cloned.1.call-start = ((), (), s32[]{:S(2)}) async-start(), calls=%async_computation.1 | async-start | bytes 2621440 | tf_op jit(solution)/shard_map/all_gather | solution.py:28
  8.0 141.4 %all-gather.10.cloned.1.call-start = ((), (), s32[]{:S(2)}) async-start(), calls=%async_computation.3 | async-start | bytes 2621440 | tf_op jit(solution)/shard_map/all_gather | solution.py:52
  8.7 195.5 %all-reduce.4.cloned.1.call-start = ((), (), s32[]{:S(2)}) async-start(), calls=%async_computation.4 | async-start | bytes 4194304 | tf_op jit(solution)/shard_map/psum | solution.py:55
  153.9 1.4 copy-start.1
  153.9 201.5 %all-gather.12.cloned.1.call-start = ((), (), s32[]{:S(2)}) async-start(), calls=%async_computation.5 | async-start | bytes 10485760 | tf_op jit(solution)/shard_map/all_gather | solution.py:61
  154.5 350.1 %all-gather.14.cloned.1.call-start = ((), (), s32[]{:S(2)}) async-start(), calls=%async_computation.6 | async-start | bytes 10485760 | tf_op jit(solution)/shard_map/all_gather | solution.py:64
  155.1 395.7 %reduce-scatter.2.cloned.1.call-start = ((), (), s32[]{:S(2)}) async-start(), calls=%async_computation.7 | async-start | bytes 2621440 | tf_op jit(solution)/shard_map/reduce_scatter | solution.py:65
Sparse Core Ops, SparseCore 0:
  8.9 48.3 all-gather.7
  58.9 44.4 all-gather.5
  105.0 44.4 all-gather.9
  154.0 50.1 all-reduce.3
  205.6 149.6 all-gather.11
  356.8 147.7 all-gather.13
  521.4 29.3 reduce-scatter.1
where the time goes:
time: 560 us
  waiting for transfers between devices  495 us (88%)
  matrix products  26.9 us (5%)
  other arithmetic  15 us (3%)
  between operations  13.6 us (2%)
  blocking collectives  6.79 us (1%)
    all_gather x1, waiting for transfers between devices, shards(): whole_down = lax.all_gather(w_down, 'fs', axis=1, tiled=True)  149 us
    all_gather x1, waiting for transfers between devices, shards(): lax.all_gather(w_up, 'fs', axis=0, tiled=True)  147 us
    psum x1, waiting for transfers between devices, shards(): lax.psum(partial_value.astype(jnp.bfloat16), 'tp').astype(jnp.float32)  48.9 us
    all_gather x1, waiting for transfers between devices, shards(): lax.all_gather(w_value, 'fs', axis=0, tiled=True)  43 us
    all_gather x1, waiting for transfers between devices, shards(): lax.all_gather(w_gate, 'fs', axis=0, tiled=True)  42.5 us
    all_gather x1, waiting for transfers between devices, shards(): lax.all_gather(w_out, 'fs', axis=1, tiled=True)  31.4 us
    reduce_scatter x1, waiting for transfers between devices, shards(): lax.psum_scatter(jnp.dot(hidden, whole_down, preferred_element_type=jnp.f...  29.5 us
    dot_general x1, matrix products, shards(): jnp.dot(hidden, whole_down, preferred_element_type=jnp.float32)  16.6 us
  transfers between devices with their start and end apart: 7, of which 7 were waited for; matrix products, arithmetic and copies ran while one was open for 4% of the time, Pallas kernels for 0%

commit v1 on v0

--- a/solution.py
+++ b/solution.py
@@ -61,7 +61,8 @@
         columns, lax.all_gather(w_up, "fs", axis=0, tiled=True), preferred_element_type=jnp.float32
     )
     hidden = jnp.square(jax.nn.relu(up_act)).astype(jnp.bfloat16)
-    whole_down = lax.all_gather(w_down, "fs", axis=1, tiled=True)
+    placed = lax.all_gather(w_down, axis_name="fs")
+    whole_down = jnp.concatenate(placed, 1)
     mlp_own = lax.psum_scatter(
         jnp.dot(hidden, whole_down, preferred_element_type=jnp.float32).astype(jnp.bfloat16),
         "tp",

time: 560 us -> 561 us (level)
  waiting for transfers between devices: 495 us -> 482 us
  local copies, waits for them, and re-layouts: 2.49 us -> 14.2 us
    reshape x0 -> x1, local copies, waits for them, and re-layouts: none -> 11.8 us  [shards(): whole_down = jnp.concatenate(placed, 1)]
    all_gather x1, waiting for transfers between devices: 147 us -> 137 us  [shards(): lax.all_gather(w_up, 'fs', axis=0, tiled=True)]
  transfers between devices with their start and end apart: 7 -> 7, of which waited for: 7 -> 7; matrix products, arithmetic and copies ran while one was open for 4% -> 6% of each run, Pallas kernels for 0% -> 0%
where the time goes in v1:
time: 561 us; the launch traced here: 560 us
  waiting for transfers between devices  482 us (86%)
  matrix products  28.2 us (5%)
  other arithmetic  15.1 us (3%)
  local copies, waits for them, and re-layouts  14.2 us (3%)
  between operations  13.6 us (2%)
  blocking collectives  6.81 us (1%)
    all_gather x1, waiting for transfers between devices, shards(): placed = lax.all_gather(w_down, axis_name='fs')  147 us
    all_gather x1, waiting for transfers between devices, shards(): lax.all_gather(w_up, 'fs', axis=0, tiled=True)  137 us
    psum x1, waiting for transfers between devices, shards(): lax.psum(partial_value.astype(jnp.bfloat16), 'tp').astype(jnp.float32)  48.9 us
    all_gather x1, waiting for transfers between devices, shards(): lax.all_gather(w_gate, 'fs', axis=0, tiled=True)  42.5 us
    all_gather x1, waiting for transfers between devices, shards(): lax.all_gather(w_value, 'fs', axis=0, tiled=True)  42 us
    all_gather x1, waiting for transfers between devices, shards(): lax.all_gather(w_out, 'fs', axis=1, tiled=True)  31.1 us
    reduce_scatter x1, waiting for transfers between devices, shards(): lax.psum_scatter(jnp.dot(hidden, whole_down, preferred_element_type=jnp.f...  29.5 us
    dot_general x1, matrix products, shards(): jnp.dot(hidden, whole_down, preferred_element_type=jnp.float32)  16.6 us
  transfers between devices with their start and end apart: 7, of which 7 were waited for; matrix products, arithmetic and copies ran while one was open for 6% of the time, Pallas kernels for 0%

profile of v1, /device:TPU:0, one launch (start us, length us, event | category | flops | bytes accessed | tf_op | source)
XLA Modules:
  0.0 559.9 jit_solution(4631700407277298017)
XLA Ops:
  6.5 0.0 copy-start
  6.5 0.0 all-gather.9.cloned.1.call-start
  6.5 0.7 all-gather.9.cloned.1.call-update
  7.3 0.0 all-gather.7.cloned.1.call-start
  7.3 0.7 all-gather.7.cloned.1.call-update
  8.0 0.0 all-gather.11.cloned.1.call-start
  8.1 0.7 all-gather.11.cloned.1.call-update
  8.7 0.0 all-reduce.4.cloned.1.call-start
  8.8 0.7 convert_element_type.46
  9.5 0.8 dynamic-slice_convert_fusion
  10.3 1.2 fusion.50
  11.5 1.2 constant_dynamic-slice_fusion
  12.7 2.1 fusion
  14.8 42.5 %all-gather.9.cloned.1.call-done = bf16[2048,512]{1,0:T(8,128)(2,1)} async-done(((bf16[512,512]{1,0:T(8,128)(2,1)}), bf16[2048,512]{1,0:T(8,128)(2,1)}) %all-gather.9.cloned.1.call-update) | async-done | bytes 2097168 | tf_op jit(solution)/shard_map/all_gather | solution.py:33
  57.3 0.0 copy-done
  57.3 4.0 fusion.7
  61.3 42.0 %all-gather.7.cloned.1.call-done = bf16[2048,512]{1,0:T(8,128)(2,1)} async-done(((bf16[512,512]{1,0:T(8,128)(2,1)}), bf16[2048,512]{1,0:T(8,128)(2,1)}) %all-gather.7.cloned.1.call-update) | async-done | bytes 2097168 | tf_op jit(solution)/shard_map/all_gather | solution.py:28
  103.4 3.1 convolution_multiply_fusion
  106.5 5.0 fusion.49
  111.5 6.8 %all-reduce.1 = (f32[512]{0:T(512)S(1)}, f32[512]{0:T(512)S(1)}) all-reduce(f32[512]{0:T(512)S(1)} %get-tuple-element.6, f32[512]{0:T(512)S(1)} %get-tuple-element.5), channel_id=1, replica_groups=mesh['grp'=2,'fs'=4,'tp'=4] {'tp'}, use_global_device_ids=true, to_apply=%region_4.5 | all-reduce | flops 1024 | bytes 8192 | tf_op jit(solution)/shard_map/psum | solution.py:42
  118.3 31.1 %all-gather.11.cloned.1.call-done = bf16[512,2048]{1,0:T(8,128)(2,1)} async-done(((bf16[512,512]{1,0:T(8,128)(2,1)}), bf16[512,2048]{1,0:T(8,128)(2,1)}) %all-gather.11.cloned.1.call-update) | async-done | bytes 2097168 | tf_op jit(solution)/shard_map/all_gather | solution.py:52
  149.5 4.4 convolution_convert_fusion.1
  153.9 0.0 all-reduce.4.cloned.1.call-update
  153.9 0.0 copy-start.1
  153.9 0.0 all-gather.15.cloned.1.call-start
  153.9 0.5 all-gather.15.cloned.1.call-update
  154.5 0.0 all-gather.13.cloned.1.call-start
  154.5 0.5 all-gather.13.cloned.1.call-update
  155.1 0.2 reduce-scatter.2.cloned.1.call-start
  155.3 0.0 copy-done.1
  155.3 48.9 %all-reduce.4.cloned.1.call-done = bf16[512,2048]{1,0:T(8,128)(2,1)} async-done(((bf16[512,2048]{1,0:T(8,128)(2,1)}), bf16[512,2048]{1,0:T(8,128)(2,1)}) %all-reduce.4.cloned.1.call-update) | async-done | bytes 2097168 | tf_op jit(solution)/shard_map/psum | solution.py:55
  204.2 4.2 convert_add_fusion
  208.5 146.9 %all-gather.15.cloned.1.call-done = bf16[8192,512]{1,0:T(8,128)(2,1)} async-done(((bf16[2048,512]{1,0:T(8,128)(2,1)}), bf16[8192,512]{1,0:T(8,128)(2,1)}) %all-gather.15.cloned.1.call-update) | async-done | bytes 8388624 | tf_op jit(solution)/shard_map/all_gather | solution.py:64
  355.4 11.8 %copy.12 = bf16[2048,4,512]{0,2,1:T(8,128)(2,1)} copy(bf16[2048,4,512]{2,0,1:T(8,128)(2,1)} %bitcast.45) | data formatting | bytes 16777216 | tf_op jit(solution)/shard_map/reshape | solution.py:65
  367.1 137.5 %all-gather.13.cloned.1.call-done = bf16[2048,2048]{1,0:T(8,128)(2,1)} async-done(((bf16[512,2048]{1,0:T(8,128)(2,1)}), bf16[2048,2048]{1,0:T(8,128)(2,1)}) %all-gather.13.cloned.1.call-update) | async-done | bytes 8388624 | tf_op jit(solution)/shard_map/all_gather | solution.py:61
  504.6 16.6 %convolution_convert_fusion = bf16[512,2048]{1,0:T(8,128)(2,1)} fusion(bf16[2048,2048]{0,1:T(8,128)(2,1)} %bitcast.46, bf16[2048,2048]{1,0:T(8,128)(2,1)} %all-gather.13.cloned.1.call-done, f32[2048]{0:T(1024)S(1)} %convert_element_type.53, f32[512]{0:T(512)S(1)} %add_rsqrt_fusion, bf16[512,2048]{1,0:T(8,128)(2,1)S(1)} %copy-done, ...), kind=kOutput, calls=%fused_computation.9 | convolution fusion | flops 8600420352 | bytes 23078912 | tf_op jit(solution)/shard_map/dot_general | solution.py:67
  521.2 0.0 reduce-scatter.2.cloned.1.call-update
  521.2 29.5 %reduce-scatter.2.cloned.1.call-done = bf16[128,2048]{1,0:T(8,128)(2,1)} async-done(((bf16[512,2048]{1,0:T(8,128)(2,1)}), bf16[128,2048]{1,0:T(8,128)(2,1)}) %reduce-scatter.2.cloned.1.call-update) | async-done | bytes 524304 | tf_op jit(solution)/shard_map/reduce_scatter | solution.py:66
  550.8 2.3 add_convert_fusion
  (4 shorter events, 0.0 us)
Async XLA Ops:
  6.5 50.8 %copy-start = (bf16[512,2048]{1,0:T(8,128)(2,1)S(1)}, bf16[512,2048]{1,0:T(8,128)(2,1)}, u32[]{:S(2)}) copy-start(bf16[512,2048]{1,0:T(8,128)(2,1)} %param.11) | copy-start | bytes 6291460
  6.5 50.8 %all-gather.9.cloned.1.call-start = ((), (), s32[]{:S(2)}) async-start(), calls=%async_computation.2 | async-start | bytes 2621440 | tf_op jit(solution)/shard_map/all_gather | solution.py:33
  7.3 96.1 %all-gather.7.cloned.1.call-start = ((), (), s32[]{:S(2)}) async-start(), calls=%async_computation.1 | async-start | bytes 2621440 | tf_op jit(solution)/shard_map/all_gather | solution.py:28
  8.0 141.4 %all-gather.11.cloned.1.call-start = ((), (), s32[]{:S(2)}) async-start(), calls=%async_computation.3 | async-start | bytes 2621440 | tf_op jit(solution)/shard_map/all_gather | solution.py:52
  8.7 195.5 %all-reduce.4.cloned.1.call-start = ((), (), s32[]{:S(2)}) async-start(), calls=%async_computation.4 | async-start | bytes 4194304 | tf_op jit(solution)/shard_map/psum | solution.py:55
  153.9 1.4 copy-start.1
  153.9 201.5 %all-gather.15.cloned.1.call-start = ((), (), s32[]{:S(2)}) async-start(), calls=%async_computation.7 | async-start | bytes 10485760 | tf_op jit(solution)/shard_map/all_gather | solution.py:64
  154.5 350.1 %all-gather.13.cloned.1.call-start = ((), (), s32[]{:S(2)}) async-start(), calls=%async_computation.5 | async-start | bytes 10485760 | tf_op jit(solution)/shard_map/all_gather | solution.py:61
  155.1 395.7 %reduce-scatter.2.cloned.1.call-start = ((), (), s32[]{:S(2)}) async-start(), calls=%async_computation.6 | async-start | bytes 2621440 | tf_op jit(solution)/shard_map/reduce_scatter | solution.py:66
Sparse Core Ops, SparseCore 0:
  8.9 48.3 all-gather.8
  58.9 44.4 all-gather.6
  105.0 44.4 all-gather.10
  154.0 50.1 all-reduce.3
  205.6 149.6 all-gather.14
  356.8 147.7 all-gather.12
  521.4 29.3 reduce-scatter.1
